TPU v7x, 512 devices: a whole 4x8x8 slice. The times are simulated.
512 devices in a mesh: fs: 64 (over z, y), tp: 8 (over x, core).
Axes of the slice: x: 4, y: 8, z: 8, core: 2. Of those that a mesh axis runs over, the one named last changes fastest.
Arguments:
- saved_inputs: bfloat16 [49152, 2048], P('fs'), may hold values from -16 to 16
- cotangents: bfloat16 [3, 49152, 1024], P(None, 'fs', 'tp'), may hold values from -0.02734375 to 0.02734375
- left_roots: float32 [3, 2048, 2048], P(None, 'fs'), may hold values from -1 to 2
- right_roots: float32 [3, 1024, 128], P(None, 'tp'), may hold values from -1 to 2
- moments: float32 [3, 2048, 1024], P(None, 'fs', 'tp'), may hold values from -125 to 125
- masters: float32 [3, 2048, 1024], P(None, 'fs', 'tp'), may hold values from -3 to 3
Outputs:
- direction: float32 [3, 2048, 1024], P(None, 'fs', 'tp')
- moments_new: float32 [3, 2048, 1024], P(None, 'fs', 'tp')
- copies: bfloat16 [3, 2048, 1024], P(None, None, 'tp')
All inputs are finite; a program needn't handle non-finite values.
Results may differ from a plain program's by a relative error of at most 0.002.
Values may be sent and summed in bfloat16 or wider, within the bound.
A program may use at most 64 MiB of HBM per device.

v0:
```python
import jax
import jax.numpy as jnp
from jax import lax
from jax.sharding import Mesh
from jax.sharding import PartitionSpec as P

D = 2048
SBW = 1024
RB = 128
FS = ("fs_0", "fs_1")
TP = ("tp_0", "tp_1")
momentum_decay = 0.9
step_rate = 0.1
eps_value = 1e-06


def filled_up(lines, peers):
    spare = -len(lines) % peers
    return jnp.pad(lines, [(0, spare)] + [(0, 0)] * (lines.ndim - 1))


def in_order(pieces, dim):
    lengths = list(pieces.shape[1:])
    lengths[dim] *= pieces.shape[0]
    return jnp.moveaxis(pieces, 0, dim).reshape(lengths)


def from_everyone(value, axis):
    peers = lax.axis_size(axis)
    return lax.all_to_all(
        jnp.broadcast_to(value[None], (peers, *value.shape)), axis, 0, 0, tiled=True
    )


def collect(value, axis, dim):
    return in_order(from_everyone(value, axis), dim)


def in_blocks(value, dim, peers):
    before, after = (value.shape[:dim], value.shape[dim + 1 :])
    return jnp.moveaxis(value.reshape(*before, peers, -1, *after), dim, 0)


def summed_on_arrival(value, axis, dim):
    peers = lax.axis_size(axis)
    pieces = lax.all_to_all(in_blocks(value, dim, peers), axis, 0, 0, tiled=True)
    return jnp.sum(pieces.astype(jnp.float32), axis=0)


def nested_sum(value, axes):
    lines = value.reshape(-1, value.shape[-1])
    padded = filled_up(lines, lax.axis_size(axes))
    whole = collect(summed_on_arrival(padded, axes, 0).astype(jnp.bfloat16), axes, 0)
    return lax.slice_in_dim(whole, 0, len(lines)).reshape(value.shape).astype(jnp.float32)


def taken_together(value, axis):
    everything = from_everyone(value, axis)
    return jnp.sum(everything, axis=0)


def by_axis(value, axes):
    far, near = axes
    nearer = taken_together(value, near)
    return taken_together(nearer, far)


def on_device(saved_inputs, cotangents, left_roots, right_roots, moments, masters):
    rows_own = masters.shape[1]
    columns = masters.shape[2]
    partial_value = jnp.einsum(
        "td,mtc->dmc", saved_inputs, cotangents, preferred_element_type=jnp.float32
    )
    summed = nested_sum(partial_value.astype(jnp.bfloat16), FS)
    left_done = jnp.einsum("mrd,dmc->mrc", left_roots, summed, precision=lax.Precision.HIGHEST)
    block_count = columns // RB
    right_blocks = right_roots.reshape(3, block_count, RB, RB)
    right_done = jnp.einsum(
        "mrbi,mbij->mrbj",
        left_done.reshape(3, rows_own, block_count, RB),
        right_blocks,
        precision=lax.Precision.HIGHEST,
    ).reshape(3, rows_own, columns)
    moments_new = momentum_decay * moments + right_done
    totals = by_axis(
        jnp.sum(moments_new * moments_new, axis=(1, 2)), (("fs_0", "fs_1"), ("tp_0", "tp_1"))
    )
    meansq = totals / (D * SBW)
    direction = moments_new * lax.rsqrt(meansq + eps_value)[:, None, None]
    copy_rows = (masters - step_rate * direction).astype(jnp.bfloat16)
    copies = lax.all_gather(copy_rows, FS, axis=1, tiled=True)
    return (direction, moments_new, copies)


def solution(mesh):
    torus = Mesh(mesh.devices.reshape(8, 8, 4, 2), ("fs_0", "fs_1", "tp_0", "tp_1"))
    in_specs = (
        P(FS, None),
        P(None, FS, TP),
        P(None, FS, None),
        P(None, TP, None),
        P(None, FS, TP),
        P(None, FS, TP),
    )
    out_specs = (P(None, FS, TP), P(None, FS, TP), P(None, None, TP))
    return jax.shard_map(
        on_device, mesh=torus, in_specs=in_specs, out_specs=out_specs, check_vma=False
    )
```

profile of v0, /device:TPU:2, one launch (start us, length us, event | category | flops | bytes accessed | tf_op | source)
XLA Modules:
  0.0 252.0 jit_solution(6863095140001499343)
XLA Ops:
  7.2 0.0 copy-start
  7.2 0.0 all-gather.2.cloned.1.call-start
  7.2 1.8 copy-done
  9.1 2.9 %fusion.2 = bf16[2048,3,128]{2,0,1:T(8,128)(2,1)S(1)} fusion(bf16[3,768,128]{2,1,0:T(8,128)(2,1)} %param.7, bf16[768,2048]{1,0:T(8,128)(2,1)S(1)} %copy-done), kind=kOutput, calls=%fused_computation.2 | convolution fusion | flops 1208745984 | bytes 5308416 | tf_op jit(solution)/shard_map/td,mtc->dmc/dot_general | solution.py:71
  12.0 10.8 %copy.21 = bf16[2048,3,128]{2,1,0:T(4,128)(2,1)} copy(bf16[2048,3,128]{2,0,1:T(8,128)(2,1)S(1)} %fusion.2) | data formatting | bytes 3145728 | tf_op jit(solution)/shard_map/convert_element_type | solution.py:74
  22.7 5.0 %reshape.37 = bf16[64,96,128]{2,1,0:T(8,128)(2,1)} reshape(bf16[2048,3,128]{2,1,0:T(4,128)(2,1)} %copy.21) | data formatting | bytes 3145728 | tf_op jit(solution)/shard_map/reshape | solution.py:41
  27.8 58.0 %all_to_all.22 = bf16[64,96,128]{2,1,0:T(8,128)(2,1)} all-to-all(bf16[64,96,128]{2,1,0:T(8,128)(2,1)} %reshape.37), channel_id=1, replica_groups=mesh['fs_0'=8,'fs_1'=8,'tp_0'=4,'tp_1'=2] {'fs_0','fs_1'}, dimensions={0} | all-to-all | bytes 3145728 | tf_op jit(solution)/shard_map/all_to_all | solution.py:46
  85.8 1.7 reduce_sum.39
  87.4 0.2 broadcast_in_dim.6
  87.6 47.3 %all_to_all.23 = bf16[64,96,128]{2,1,0:T(8,128)(2,1)} all-to-all(bf16[64,96,128]{2,1,0:T(8,128)(2,1)S(1)} %broadcast_in_dim.6), channel_id=1, replica_groups=mesh['fs_0'=8,'fs_1'=8,'tp_0'=4,'tp_1'=2] {'fs_0','fs_1'}, dimensions={0} | all-to-all | bytes 3145728 | tf_op jit(solution)/shard_map/all_to_all | solution.py:30
  134.9 5.2 %reshape_reshape.3 = bf16[2048,3,128]{2,1,0:T(4,128)(2,1)} reshape(bf16[64,96,128]{2,1,0:T(8,128)(2,1)} %all_to_all.23) | data formatting | bytes 3145728 | tf_op jit(solution)/shard_map/reshape;reshape | solution.py:54
  140.1 2.6 %fusion.5 = f32[3,128,32]{1,2,0:T(8,128)S(1)} fusion(f32[3,32,2048]{2,1,0:T(8,128)} %param.8, bf16[2048,3,128]{2,1,0:T(4,128)(2,1)} %reshape_reshape.3), kind=kOutput, calls=%fused_computation.3 | convolution fusion | flops 301989888 | bytes 2408448 | tf_op jit(solution)/shard_map/mrd,dmc->mrc/dot_general | solution.py:75
  142.7 0.0 copy-done.1
  142.7 0.0 copy-done.4
  142.8 0.4 multiply_reduce_fusion
  143.1 8.5 %all_to_all.24 = f32[8,1,3]{2,1,0:T(1,128)S(1)} all-to-all(f32[8,1,3]{2,1,0:T(1,128)S(1)} %broadcast_in_dim.7), channel_id=1, replica_groups=mesh['fs_0'=8,'fs_1'=8,'tp_0'=4,'tp_1'=2] {'tp_0','tp_1'}, dimensions={0} | all-to-all | bytes 192 | tf_op jit(solution)/shard_map/all_to_all | solution.py:30
  151.7 18.5 %all_to_all.25 = f32[64,1,3]{2,1,0:T(1,128)S(1)} all-to-all(f32[64,1,3]{2,1,0:T(1,128)S(1)} %broadcast_in_dim.8), channel_id=1, replica_groups=mesh['fs_0'=8,'fs_1'=8,'tp_0'=4,'tp_1'=2] {'fs_0','fs_1'}, dimensions={0} | all-to-all | bytes 1536 | tf_op jit(solution)/shard_map/all_to_all | solution.py:30
  170.2 0.1 reduce_sum.42
  170.3 0.0 copy-done.3
  170.3 0.7 subtract_convert_fusion
  171.0 0.0 all-gather.2.cloned.1.call-update
  171.0 71.5 %all-gather.2.cloned.1.call-done = bf16[3,2048,128]{2,1,0:T(8,128)(2,1)} async-done(((bf16[3,32,128]{2,1,0:T(8,128)(2,1)}), bf16[3,2048,128]{2,1,0:T(8,128)(2,1)}) %all-gather.2.cloned.1.call-update) | async-done | bytes 1572880 | tf_op jit(solution)/shard_map/all_gather | solution.py:91
  242.5 2.7 %copy.32 = bf16[3,2048,128]{2,1,0:T(8,128)(2,1)} copy(bf16[3,2048,128]{2,1,0:T(8,128)(2,1)} %all-gather.2.cloned.1.call-done) | data formatting | bytes 3145728
  245.2 0.0 copy-done.2
  (8 shorter events, 0.1 us)
Async XLA Ops:
  7.2 1.9 copy-start
  7.2 235.3 %all-gather.2.cloned.1.call-start = ((), (), s32[]{:S(2)}) async-start(), calls=%async_computation.4 | async-start | bytes 1597440 | tf_op jit(solution)/shard_map/all_gather | solution.py:91
  140.1 2.6 %copy-start.1 = (f32[3,128,128]{2,1,0:T(8,128)S(1)}, f32[3,128,128]{2,1,0:T(8,128)}, u32[]{:S(2)}) copy-start(f32[3,128,128]{2,1,0:T(8,128)} %param.9) | copy-start | bytes 589828
  140.1 2.7 %copy-start.4 = (f32[3,32,128]{2,1,0:T(8,128)S(1)}, f32[3,32,128]{2,1,0:T(8,128)}, u32[]{:S(2)}) copy-start(f32[3,32,128]{2,1,0:T(8,128)} %param.10) | copy-start | bytes 147460
  140.1 30.2 %copy-start.3 = (f32[3,32,128]{2,1,0:T(8,128)S(1)}, f32[3,32,128]{2,1,0:T(8,128)}, u32[]{:S(2)}) copy-start(f32[3,32,128]{2,1,0:T(8,128)} %param.11) | copy-start | bytes 147460
  143.1 102.0 %copy-start.2 = (f32[3,32,128]{2,1,0:T(8,128)}, f32[3,32,128]{2,1,0:T(8,128)S(1)}, u32[]{:S(2)}) copy-start(f32[3,32,128]{2,1,0:T(8,128)S(1)} %get-tuple-element.11) | copy-start | bytes 147460
Sparse Core Ops, SparseCore 0:
  171.1 71.3 all-gather.1
where the time goes:
time: 253 us; the launch traced here: 252 us
  blocking collectives  132 us (52%)
  waiting for transfers between devices  71.5 us (28%)
  local copies, waits for them, and re-layouts  25.7 us (10%)
  between operations  14.1 us (6%)
  matrix products  5.9 us (2%)
    all_to_all x3, blocking collectives, from_everyone(): lax.all_to_all(jnp.broadcast_to(value[None], (peers, *value.shape)), axis...  74.3 us
    all_gather x1, waiting for transfers between devices, on_device(): copies = lax.all_gather(copy_rows, FS, axis=1, tiled=True)  71.5 us
    all_to_all x1, blocking collectives, summed_on_arrival(): lax.all_to_all(in_blocks(value, dim, peers), axis, 0, 0, tiled=True)  58 us
    convert_element_type x1, local copies, waits for them, and re-layouts, on_device(): summed = nested_sum(partial_value.astype(jnp.bfloat16), FS)  10.8 us
    another operation x1, local copies, waits for them, and re-layouts, nested_sum(): lax.slice_in_dim(whole, 0, len(lines)).reshape(value.shape)  5.19 us
  transfers between devices with their start and end apart: 1, of which 1 were waited for; matrix products, arithmetic and copies ran while one was open for 0% of the time, Pallas kernels for 0%

commit v1 on v0

--- a/solution.py
+++ b/solution.py
@@ -1,3 +1,4 @@
+import functools
 import jax
 import jax.numpy as jnp
 from jax import lax
@@ -12,6 +13,21 @@
 momentum_decay = 0.9
 step_rate = 0.1
 eps_value = 1e-06
+
+
+def remake_columns(local_x, a_name, array_axis):
+    return jnp.concatenate(
+        lax.all_to_all(
+            jnp.stack(tuple((local_x for _ in range(lax.axis_size(a_name))))),
+            axis_name=a_name,
+            split_axis=0,
+            concat_axis=0,
+        ),
+        array_axis,
+    )
+
+
+obtain_loads = functools.partial(remake_columns, a_name=FS, array_axis=1)
 
 
 def filled_up(lines, peers):
@@ -88,7 +104,7 @@
     meansq = totals / (D * SBW)
     direction = moments_new * lax.rsqrt(meansq + eps_value)[:, None, None]
     copy_rows = (masters - step_rate * direction).astype(jnp.bfloat16)
-    copies = lax.all_gather(copy_rows, FS, axis=1, tiled=True)
+    copies = obtain_loads(copy_rows)
     return (direction, moments_new, copies)
 
 

time: 253 us -> 211 us (0.83)
  the two profiles are of different devices: /device:TPU:2 before, /device:TPU:8 now
where the time goes in v1:
time: 211 us; the launch traced here: 210 us
  blocking collectives  176 us (83%)
  local copies, waits for them, and re-layouts  24.7 us (12%)
  matrix products  5.91 us (3%)
  other arithmetic  2.47 us (1%)
    all_to_all x3, blocking collectives, from_everyone(): lax.all_to_all(jnp.broadcast_to(value[None], (peers, *value.shape)), axis...  74.6 us
    all_to_all x1, blocking collectives, summed_on_arrival(): lax.all_to_all(in_blocks(value, dim, peers), axis, 0, 0, tiled=True)  57.5 us
    all_to_all x1, blocking collectives, remake_columns(): lax.all_to_all(jnp.stack(tuple((local_x for _ in range(lax.axis_size(a_na...  44.3 us
    convert_element_type x1, local copies, waits for them, and re-layouts, on_device(): summed = nested_sum(partial_value.astype(jnp.bfloat16), FS)  10.8 us
    another operation x1, local copies, waits for them, and re-layouts, nested_sum(): lax.slice_in_dim(whole, 0, len(lines)).reshape(value.shape)  5.19 us
    reshape x1, local copies, waits for them, and re-layouts, in_blocks(): return jnp.moveaxis(value.reshape(*before, peers, -1, *after), dim, 0)  5.01 us

profile of v1, /device:TPU:8, one launch (start us, length us, event | category | flops | bytes accessed | tf_op | source)
XLA Modules:
  0.0 210.3 jit_solution(839805300357958177)
XLA Ops:
  0.6 0.0 copy-start
  0.6 1.9 copy-done
  2.5 2.9 %fusion.2 = bf16[2048,3,128]{2,0,1:T(8,128)(2,1)S(1)} fusion(bf16[3,768,128]{2,1,0:T(8,128)(2,1)} %param.7, bf16[768,2048]{1,0:T(8,128)(2,1)S(1)} %copy-done), kind=kOutput, calls=%fused_computation.2 | convolution fusion | flops 1208745984 | bytes 5308416 | tf_op jit(solution)/shard_map/td,mtc->dmc/dot_general | solution.py:87
  5.4 10.8 %copy.30 = bf16[2048,3,128]{2,1,0:T(4,128)(2,1)} copy(bf16[2048,3,128]{2,0,1:T(8,128)(2,1)S(1)} %fusion.2) | data formatting | bytes 3145728 | tf_op jit(solution)/shard_map/convert_element_type | solution.py:90
  16.2 5.0 %reshape.45 = bf16[64,96,128]{2,1,0:T(8,128)(2,1)} reshape(bf16[2048,3,128]{2,1,0:T(4,128)(2,1)} %copy.30) | data formatting | bytes 3145728 | tf_op jit(solution)/shard_map/reshape | solution.py:57
  21.2 57.5 %all_to_all.27 = bf16[64,96,128]{2,1,0:T(8,128)(2,1)} all-to-all(bf16[64,96,128]{2,1,0:T(8,128)(2,1)} %reshape.45), channel_id=1, replica_groups=mesh['fs_0'=8,'fs_1'=8,'tp_0'=4,'tp_1'=2] {'fs_0','fs_1'}, dimensions={0} | all-to-all | bytes 3145728 | tf_op jit(solution)/shard_map/all_to_all | solution.py:62
  78.8 1.7 reduce_sum.39
  80.4 0.2 broadcast_in_dim.6
  80.6 47.3 %all_to_all.28 = bf16[64,96,128]{2,1,0:T(8,128)(2,1)} all-to-all(bf16[64,96,128]{2,1,0:T(8,128)(2,1)S(1)} %broadcast_in_dim.6), channel_id=1, replica_groups=mesh['fs_0'=8,'fs_1'=8,'tp_0'=4,'tp_1'=2] {'fs_0','fs_1'}, dimensions={0} | all-to-all | bytes 3145728 | tf_op jit(solution)/shard_map/all_to_all | solution.py:46
  127.9 5.2 %reshape_reshape.3 = bf16[2048,3,128]{2,1,0:T(4,128)(2,1)} reshape(bf16[64,96,128]{2,1,0:T(8,128)(2,1)} %all_to_all.28) | data formatting | bytes 3145728 | tf_op jit(solution)/shard_map/reshape;reshape | solution.py:70
  133.1 0.0 copy-start.1
  133.1 2.6 %fusion.5 = f32[3,128,32]{1,2,0:T(8,128)S(1)} fusion(f32[3,32,2048]{2,1,0:T(8,128)} %param.8, bf16[2048,3,128]{2,1,0:T(4,128)(2,1)} %reshape_reshape.3), kind=kOutput, calls=%fused_computation.3 | convolution fusion | flops 301989888 | bytes 2408448 | tf_op jit(solution)/shard_map/mrd,dmc->mrc/dot_general | solution.py:91
  135.8 0.0 copy-done.1
  135.8 0.0 copy-done.4
  135.8 0.4 multiply_reduce_fusion
  136.2 9.4 %all_to_all.29 = f32[8,1,3]{2,1,0:T(1,128)S(1)} all-to-all(f32[8,1,3]{2,1,0:T(1,128)S(1)} %broadcast_in_dim.7), channel_id=1, replica_groups=mesh['fs_0'=8,'fs_1'=8,'tp_0'=4,'tp_1'=2] {'tp_0','tp_1'}, dimensions={0} | all-to-all | bytes 192 | tf_op jit(solution)/shard_map/all_to_all | solution.py:46
  145.6 17.9 %all_to_all.30 = f32[64,1,3]{2,1,0:T(1,128)S(1)} all-to-all(f32[64,1,3]{2,1,0:T(1,128)S(1)} %broadcast_in_dim.8), channel_id=1, replica_groups=mesh['fs_0'=8,'fs_1'=8,'tp_0'=4,'tp_1'=2] {'fs_0','fs_1'}, dimensions={0} | all-to-all | bytes 1536 | tf_op jit(solution)/shard_map/all_to_all | solution.py:46
  163.5 0.1 reduce_sum.42
  163.6 0.0 copy-done.3
  163.6 0.7 subtract_convert_fusion
  164.3 0.2 stack.2
  164.5 44.3 %all_to_all.31 = bf16[64,3,32,128]{3,2,1,0:T(8,128)(2,1)S(1)} all-to-all(bf16[64,3,32,128]{3,2,1,0:T(8,128)(2,1)S(1)} %stack.2), channel_id=1, replica_groups=mesh['fs_0'=8,'fs_1'=8,'tp_0'=4,'tp_1'=2] {'fs_0','fs_1'}, dimensions={0} | all-to-all | bytes 3145728 | tf_op jit(solution)/shard_map/all_to_all | solution.py:20
  208.9 0.0 copy-done.2
  208.9 1.4 copy.34
  (7 shorter events, 0.1 us)
Async XLA Ops:
  0.6 1.9 copy-start
  133.1 2.6 %copy-start.1 = (f32[3,128,128]{2,1,0:T(8,128)S(1)}, f32[3,128,128]{2,1,0:T(8,128)}, u32[]{:S(2)}) copy-start(f32[3,128,128]{2,1,0:T(8,128)} %param.9) | copy-start | bytes 589828
  133.1 2.7 %copy-start.4 = (f32[3,32,128]{2,1,0:T(8,128)S(1)}, f32[3,32,128]{2,1,0:T(8,128)}, u32[]{:S(2)}) copy-start(f32[3,32,128]{2,1,0:T(8,128)} %param.10) | copy-start | bytes 147460
  133.1 30.5 %copy-start.3 = (f32[3,32,128]{2,1,0:T(8,128)S(1)}, f32[3,32,128]{2,1,0:T(8,128)}, u32[]{:S(2)}) copy-start(f32[3,32,128]{2,1,0:T(8,128)} %param.11) | copy-start | bytes 147460
  136.1 72.7 %copy-start.2 = (f32[3,32,128]{2,1,0:T(8,128)}, f32[3,32,128]{2,1,0:T(8,128)S(1)}, u32[]{:S(2)}) copy-start(f32[3,32,128]{2,1,0:T(8,128)S(1)} %get-tuple-element.6) | copy-start | bytes 147460
